TPU v7x, 32 devices: a whole 2x2x4 slice. The times are simulated.
32 devices in a mesh: ep: 8 (over z, x), tp: 4 (over y, core).
Axes of the slice: x: 2, y: 2, z: 4, core: 2. Of those that a mesh axis runs over, the one named last changes fastest.
Arguments:
- tokens: bfloat16 [64, 2048], P('ep'), may hold values from -6 to 6
- norm_gain: float32 [2048], replicated, may hold values from 0.1 to 1.9
- query_weight: bfloat16 [2048, 1024], P('ep', 'tp'), may hold values from -0.125 to 0.125
- key_weight: bfloat16 [2048, 512], P('ep', 'tp'), may hold values from -0.125 to 0.125
- value_weight: bfloat16 [2048, 512], P('ep', 'tp'), may hold values from -0.125 to 0.125
- query_gain: float32 [64], replicated, may hold values from 0.9 to 1.9
- key_gain: float32 [64], replicated, may hold values from 0.9 to 1.9
- lambdas: float32 [8], P('tp'), may hold values from 0.3 to 0.8
- key_cache: bfloat16 [64, 4, 320, 128], P('ep', 'tp'), may hold values from -5 to 5
- value_cache: bfloat16 [64, 4, 320, 128], P('ep', 'tp'), may hold values from -6 to 6
- lengths: int32 [64], P('ep'), may hold values from 1 to 320
- head_gain: float32 [128], replicated, may hold values from 0.1 to 1.9
- out_weight: bfloat16 [1024, 2048], P('tp', 'ep'), may hold values from -0.1875 to 0.1875
- ffn_gain: float32 [2048], replicated, may hold values from 0.1 to 1.9
- dense_gate_weight: bfloat16 [2048, 1024], P('ep', 'tp'), may hold values from -0.125 to 0.125
- dense_up_weight: bfloat16 [2048, 1024], P('ep', 'tp'), may hold values from -0.125 to 0.125
- dense_down_weight: bfloat16 [1024, 2048], P('tp', 'ep'), may hold values from -0.1875 to 0.1875
- branch_gate: float32 [2048], replicated, may hold values from -0.125 to 0.125
- expert_ids: int32 [64, 2], P('ep'), may hold values from 0 to 15, all different within a row; in each aligned block of 8 rows (0 to 7, 8 to 15, ...) at most 2 rows name the same one
- expert_probs: float32 [64, 2], P('ep'), may hold values from 0.1 to 0.9
- expert_gate: bfloat16 [16, 2048, 5632], P('ep', None, 'tp'), may hold values from -0.125 to 0.125
- expert_up: bfloat16 [16, 2048, 5632], P('ep', None, 'tp'), may hold values from -0.125 to 0.125
- expert_down: bfloat16 [16, 5632, 2048], P('ep', 'tp'), may hold values from -0.078125 to 0.078125
Outputs:
- mixed: bfloat16 [64, 2048], P('ep', 'tp')
Inputs may be any that keep to these rules, and one draw needn't show every extreme that they name: `expert_ids`: each row names 2 different experts. Within each aligned block of 8 rows (the sequences of one index of ep) no expert is named more than 2 times, and in every draw some block names some expert exactly 2 times.
All inputs are finite; a program needn't handle non-finite values.
Results may differ from a plain program's by a relative error of at most 0.014.
Values may be sent and summed in bfloat16 or wider, within the bound.
A program may use at most 128 MiB of HBM per device.

v0:
```python
import functools

import jax
import jax.numpy as jnp
import numpy as np
from jax import lax
from jax.experimental import pallas as pl
from jax.experimental.pallas import tpu as pltpu
from jax.sharding import PartitionSpec as P

SUB = 64
VD = 128
EXPERTS = 16
TOP = 2
CAP = 2


epsilon = 1e-06


def rms_scale(values, scaling):
    return values * lax.rsqrt(jnp.mean(values * values, axis=-1, keepdims=True) + epsilon) * scaling


def project_rows(normed, weights):
    ep_count = lax.axis_size("ep")
    seq_here = normed.shape[0]
    stacked = jnp.concatenate(weights, axis=1)
    columns = lax.all_to_all(normed, "ep", split_axis=1, concat_axis=0, tiled=True)
    partial_value = jnp.dot(columns, stacked, preferred_element_type=jnp.float32).astype(jnp.bfloat16)
    received = lax.all_to_all(partial_value, "ep", split_axis=0, concat_axis=0, tiled=True)
    received = received.reshape(ep_count, seq_here, stacked.shape[1])
    return jnp.sum(received.astype(jnp.float32), axis=0)


def project_back(operand, weight):
    tp_count = lax.axis_size("tp")
    seq_here = operand.shape[0]
    every_row = lax.all_gather(operand, "ep", axis=0, tiled=True)
    partial_value = jnp.dot(every_row, weight, preferred_element_type=jnp.float32).astype(jnp.bfloat16)
    rows = lax.all_to_all(partial_value, "ep", split_axis=0, concat_axis=1, tiled=True)
    pieces = lax.all_to_all(rows, "tp", split_axis=1, concat_axis=0, tiled=True)
    pieces = pieces.reshape(tp_count, seq_here, pieces.shape[1])
    return jnp.sum(pieces.astype(jnp.float32), axis=0)


def attend(packed, key_cache, value_cache, lengths, query_gain, key_gain, lambdas, head_gain):
    seq_here = packed.shape[0]
    kv_here = key_cache.shape[1]
    cache_len = key_cache.shape[2]
    heads_here = lambdas.shape[0]
    per_group = heads_here // kv_here
    query_end = heads_here * 2 * SUB
    key_end = query_end + kv_here * 2 * SUB
    mixed = lax.optimization_barrier(packed.astype(jnp.bfloat16))
    query_parts = rms_scale(
        mixed[:, :query_end].astype(jnp.float32).reshape(seq_here, kv_here, per_group, 2, SUB),
        query_gain,
    ).astype(jnp.bfloat16)
    key_parts = rms_scale(
        mixed[:, query_end:key_end].astype(jnp.float32).reshape(seq_here, kv_here, 2, SUB), key_gain
    ).astype(jnp.bfloat16)
    new_values = mixed[:, key_end:].reshape(seq_here, kv_here, VD)
    cached = rms_scale(
        key_cache.astype(jnp.float32).reshape(seq_here, kv_here, cache_len, 2, SUB), key_gain
    ).astype(jnp.bfloat16)
    score_scale = SUB ** (-0.5)
    scores = (
        jnp.einsum("sgqcd,sgjcd->sgqcj", query_parts, cached, preferred_element_type=jnp.float32)
        * score_scale
    )
    own_score = (
        jnp.einsum("sgqcd,sgcd->sgqc", query_parts, key_parts, preferred_element_type=jnp.float32)
        * score_scale
    )
    live_mask = lax.broadcasted_iota(jnp.int32, (seq_here, cache_len), 1) < lengths[:, None]
    exponent = jnp.where(live_mask[:, None, None, None, :], jnp.exp(scores), 0.0)
    own_exponent = jnp.exp(own_score)
    denominator = jnp.sum(exponent, axis=4) + own_exponent
    shares = exponent / denominator[..., None]
    own_shares = own_exponent / denominator
    lam_heads = lambdas.reshape(1, kv_here, per_group)
    mixing = (shares[:, :, :, 0] - lam_heads[..., None] * shares[:, :, :, 1]).astype(jnp.bfloat16)
    own_mixing = lax.optimization_barrier(
        (own_shares[:, :, :, 0] - lam_heads * own_shares[:, :, :, 1]).astype(jnp.bfloat16)
    )
    head_out = jnp.einsum(
        "sgqj,sgje->sgqe", mixing, value_cache, preferred_element_type=jnp.float32
    )
    head_out = (
        head_out
        + own_mixing.astype(jnp.float32)[..., None] * new_values.astype(jnp.float32)[:, :, None, :]
    )
    return rms_scale(head_out, head_gain).astype(jnp.bfloat16).reshape(seq_here, heads_here * VD)


def route_tables(expert_ids, expert_probs):
    seq_here = expert_ids.shape[0]
    paired = expert_ids.reshape(-1)
    total_pairs = paired.shape[0]
    onehot = (paired[:, None] == lax.broadcasted_iota(jnp.int32, (total_pairs, EXPERTS), 1)).astype(
        jnp.float32
    )
    earlier = (
        lax.broadcasted_iota(jnp.int32, (total_pairs, total_pairs), 1)
        < lax.broadcasted_iota(jnp.int32, (total_pairs, total_pairs), 0)
    ).astype(jnp.float32)
    before = jnp.dot(earlier, onehot, precision=lax.Precision.HIGHEST)
    slot_ranks = jnp.sum(before * onehot, axis=1).astype(jnp.int32)
    slot_codes = (paired * CAP + slot_ranks).reshape(seq_here, TOP)
    slots_iota = lax.broadcasted_iota(jnp.int32, (seq_here, TOP, EXPERTS * CAP), 2)
    picked = (slot_codes[:, :, None] == slots_iota).astype(jnp.float32)
    select = jnp.sum(picked, axis=1)
    combine_weights = jnp.sum(picked * expert_probs[:, :, None], axis=1)
    return (select, combine_weights)


def mixture(ffn_input, expert_ids, expert_probs, expert_gate, expert_up, expert_down):
    here_count = expert_gate.shape[0]
    ep_count = lax.axis_size("ep")
    tp_count = lax.axis_size("tp")
    slot_count = ep_count * here_count
    rep_count = slot_count // EXPERTS
    model_width = ffn_input.shape[1]
    feature_share = model_width // tp_count
    select, combine_weights = route_tables(expert_ids, expert_probs)
    sent_width = ffn_input.shape[1]
    chosen = jnp.einsum(
        "sk,sd->kd", select.astype(jnp.bfloat16), ffn_input, preferred_element_type=jnp.float32
    ).astype(jnp.bfloat16)
    outgoing = jnp.broadcast_to(
        chosen.reshape(1, EXPERTS, CAP, sent_width), (rep_count, EXPERTS, CAP, sent_width)
    ).reshape(slot_count, CAP, sent_width)
    incoming = lax.all_to_all(outgoing, "ep", split_axis=0, concat_axis=0, tiled=True)
    grouped = incoming.reshape(ep_count, here_count, incoming.shape[1], model_width)
    gate_val = jnp.einsum(
        "ihcd,hdf->ihcf", grouped, expert_gate, preferred_element_type=jnp.float32
    )
    up_val = jnp.einsum("ihcd,hdf->ihcf", grouped, expert_up, preferred_element_type=jnp.float32)
    hidden = (jax.nn.silu(gate_val) * up_val).astype(jnp.bfloat16)
    partial_value = jnp.einsum(
        "ihcf,hfd->ihcd", hidden, expert_down, preferred_element_type=jnp.float32
    ).astype(jnp.bfloat16)
    summed = lax.all_to_all(partial_value, "tp", split_axis=3, concat_axis=0, tiled=True)
    block_out = jnp.sum(
        summed.reshape(tp_count, ep_count, here_count, CAP, feature_share).astype(jnp.float32),
        axis=0,
    ).astype(jnp.bfloat16)
    returned = lax.all_to_all(block_out, "ep", split_axis=0, concat_axis=0, tiled=True)
    expert_out = jnp.sum(
        returned.reshape(rep_count, EXPERTS * CAP, feature_share).astype(jnp.float32), axis=0
    )
    return jnp.dot(combine_weights, expert_out, precision=lax.Precision.HIGHEST)


def own_columns(values, tp_start, share_width):
    return lax.dynamic_slice_in_dim(values, tp_start, share_width, 1)


def shards(
    tokens,
    norm_gain,
    query_weight,
    key_weight,
    value_weight,
    query_gain,
    key_gain,
    lambdas,
    key_cache,
    value_cache,
    lengths,
    head_gain,
    out_weight,
    ffn_gain,
    dense_gate_weight,
    dense_up_weight,
    dense_down_weight,
    branch_gate,
    expert_ids,
    expert_probs,
    expert_gate,
    expert_up,
    expert_down,
):
    residual = tokens.astype(jnp.float32)
    normed = rms_scale(residual, norm_gain).astype(jnp.bfloat16)
    packed = project_rows(normed, (query_weight, key_weight, value_weight))
    head_out = attend(
        packed, key_cache, value_cache, lengths, query_gain, key_gain, lambdas, head_gain
    )
    attended = project_back(head_out, out_weight)
    share_width = attended.shape[1]
    tp_start = lax.axis_index("tp") * share_width
    middle_own = (own_columns(residual, tp_start, share_width) + attended).astype(jnp.bfloat16)
    middle = lax.all_gather(middle_own, "tp", axis=1, tiled=True)
    middle_f32 = middle.astype(jnp.float32)
    ffn_input = lax.optimization_barrier(rms_scale(middle_f32, ffn_gain).astype(jnp.bfloat16))
    dense_both = project_rows(ffn_input, (dense_gate_weight, dense_up_weight))
    half_width = dense_both.shape[1] // 2
    hidden = (jax.nn.silu(dense_both[:, :half_width]) * dense_both[:, half_width:]).astype(
        jnp.bfloat16
    )
    dense = project_back(hidden, dense_down_weight)
    branch_weight = jax.nn.sigmoid(
        jnp.sum(ffn_input.astype(jnp.float32) * branch_gate, axis=1, keepdims=True)
    )
    routed = mixture(ffn_input, expert_ids, expert_probs, expert_gate, expert_up, expert_down)
    combined = middle_own.astype(jnp.float32) + branch_weight * dense + routed
    return combined.astype(jnp.bfloat16)


BF = jnp.bfloat16
F32 = jnp.float32
HI = lax.Precision.HIGHEST


def contract(left, right, dims, precision=None):
    return lax.dot_general(
        left, right, ((dims[0:1], dims[1:2]), ((), ())), precision=precision, preferred_element_type=F32
    )


def silu(values):
    return values / (1.0 + jnp.exp(-values))


def layer_kernel(
    n_ep, n_tp, lam_ref, tok_ref, ngain_ref, wq_ref, wk_ref, wv_ref, qgain_ref, kgain_ref, kc_ref, vc_ref,
    len_ref, hgain_ref, wo_ref, fgain_ref, wdg_ref, wdu_ref, wdd_ref, bgate_ref, ids_ref, probs_ref,
    slot_ref, code_ref, eg_ref, eu_ref, ed_ref, out_ref,
    eg, eu, ed, kn, a_send, a_recv, b_send, b_recv, c_send, c_recv, d_send, d_recv, e_send, e_recv,
    f_send, f_recv, n_send, n_recv, i_send, i_recv, j_send, j_recv, k_send, k_recv, g_send, g_recv,
    h_send, h_recv, x_all, total, r_slot, r_rows, b_rows, wsem, ssem, rsem,
):
    e = lax.axis_index("ep")
    t = lax.axis_index("tp")
    rows, width = tok_ref.shape
    cols = width // n_ep
    seqs = rows * n_ep
    here = eg.shape[0]
    hidden_here = eg.shape[2]
    cache_len = kc_ref.shape[0] // rows
    heads = wq_ref.shape[1] // (2 * SUB)
    per_dest = here * CAP
    share = width // n_tp
    half = wdg_ref.shape[1]

    weight_copies = []
    for h in range(here):
        group = []
        for n, (src, dst) in enumerate(((eg_ref, eg), (eu_ref, eu), (ed_ref, ed))):
            copy = pltpu.make_async_copy(src.at[h], dst.at[h], wsem.at[h, n])
            copy.start()
            group.append(copy)
        weight_copies.append(group)

    barrier = pltpu.get_barrier_semaphore()
    for k in range(1, n_ep):
        pl.semaphore_signal(
            barrier, inc=1, device_id={"ep": lax.rem(e + k, n_ep)}, device_id_type=pl.DeviceIdType.MESH
        )
    for k in range(1, n_tp):
        pl.semaphore_signal(
            barrier, inc=1, device_id={"tp": lax.rem(t + k, n_tp)}, device_id_type=pl.DeviceIdType.MESH
        )

    pending = []

    def exchange(stage, axis, send, recv, sliced):
        count, me = (n_ep, e) if axis == "ep" else (n_tp, t)
        copies = []
        for k in range(1, count):
            peer = lax.rem(me + k, count)
            copy = pltpu.make_async_remote_copy(
                src_ref=send.at[peer] if sliced else send,
                dst_ref=recv.at[me],
                send_sem=ssem.at[stage, k],
                recv_sem=rsem.at[stage, k],
                device_id={axis: peer},
                device_id_type=pl.DeviceIdType.MESH,
            )
            copy.start()
            copies.append(copy)
        pending.extend(copies)
        recv[me] = send[me] if sliced else send[...]
        return copies

    def arrive(copies):
        for copy in copies:
            copy.wait_recv()

    def stack_rows(ref):
        values = ref[...].astype(F32)
        return values.reshape(values.shape[0] * values.shape[1], values.shape[2])

    tok = tok_ref[...].astype(F32)
    normed = rms_scale(tok, ngain_ref[...]).astype(BF)
    ids = ids_ref[...]
    lower = (
        lax.broadcasted_iota(jnp.int32, (rows, rows), 1) < lax.broadcasted_iota(jnp.int32, (rows, rows), 0)
    ).astype(F32)

    def placed(table):
        expert = table[0:1, :]
        hits = [(ids[:, k : k + 1] == expert).astype(F32) for k in range(TOP)]
        named = hits[0]
        for hit in hits[1:]:
            named = named + hit
        before = jnp.dot(lower, named, precision=HI, preferred_element_type=F32)
        ranked = (before == table[1:2, :].astype(F32)).astype(F32)
        return [hit * ranked for hit in hits]

    slots = slot_ref[...]
    marks = placed(slots)
    chosen = functools.reduce(lambda x, y: x + y, marks) * (slots[2:3, :] == e).astype(F32)
    chosen = chosen.astype(BF)
    code_marks = placed(code_ref[...])
    combine = functools.reduce(
        lambda x, y: x + y, [code_marks[k] * probs_ref[:, k : k + 1] for k in range(TOP)]
    )
    tok_bf = tok_ref[...]
    for d in range(n_ep):
        a_send[d, :, :cols] = normed[:, d * cols : (d + 1) * cols]
        a_send[d, :, cols : 2 * cols] = tok_bf[:, d * cols : (d + 1) * cols]
        a_send[d, :, 2 * cols :] = chosen
    pl.semaphore_wait(barrier, n_ep - 1 + n_tp - 1)
    a_copies = exchange(0, "ep", a_send, a_recv, True)

    lanes = 2 * SUB
    block = (
        (lax.broadcasted_iota(jnp.int32, (lanes, lanes), 0) < SUB)
        == (lax.broadcasted_iota(jnp.int32, (lanes, lanes), 1) < SUB)
    ).astype(F32) * (1.0 / SUB)

    def parts_norm(values, gain):
        mean = jnp.dot(values * values, block, precision=HI, preferred_element_type=F32)
        return (values * lax.rsqrt(mean + epsilon) * gain).astype(BF)

    kgain = kgain_ref[...]
    for s in range(rows):
        span = slice(s * cache_len, (s + 1) * cache_len)
        kn[span, :] = parts_norm(kc_ref[span, :].astype(F32), kgain)

    arrive(a_copies)
    stacked = stack_rows(a_recv)
    x_cols = stacked[:, :cols].astype(BF)
    tok_cols = stacked[:, cols : 2 * cols]
    dispatch = stacked[:, 2 * cols :]
    start = 0
    for w_ref in (wq_ref, wk_ref, wv_ref):
        stop = start + w_ref.shape[1]
        product = jnp.dot(x_cols, w_ref[...], preferred_element_type=F32)
        b_send[:, :, start:stop] = product.reshape(n_ep, rows, stop - start).astype(BF)
        start = stop
    arrive(exchange(1, "ep", b_send, b_recv, True))
    packed = jnp.sum(b_recv[...].astype(F32), axis=0).astype(BF).astype(F32)
    q_end = heads * lanes
    key_part = parts_norm(packed[:, q_end : q_end + lanes], kgain)
    new_value = packed[:, q_end + lanes :]
    low_half = lax.broadcasted_iota(jnp.int32, (rows, lanes), 1) < SUB
    score_scale = SUB ** (-0.5)
    stack, own = [], []
    for h in range(heads):
        query = parts_norm(packed[:, h * lanes : (h + 1) * lanes], qgain_ref[...]).astype(F32)
        own_pair = jnp.dot(
            query * key_part.astype(F32), block, precision=HI, preferred_element_type=F32
        ) * (SUB * score_scale)
        for c in range(2):
            stack.append(jnp.where(low_half if c == 0 else ~low_half, query, 0.0))
            own.append(jnp.exp(own_pair[:, c * SUB : c * SUB + 1]))
    stack = jnp.concatenate(stack, axis=0).astype(BF)
    count = 2 * heads
    row_of = lax.broadcasted_iota(jnp.int32, (count * rows, cache_len), 0) % rows
    scores = jnp.zeros((count * rows, cache_len), F32)
    for s in range(rows):
        product = contract(stack, kn[s * cache_len : (s + 1) * cache_len, :], (1, 1))
        scores = jnp.where(row_of == s, product, scores)
    live = lax.broadcasted_iota(jnp.int32, (rows, cache_len), 1) < len_ref[...]
    shares, own_shares = [], []
    for j in range(count):
        exponent = jnp.where(live, jnp.exp(scores[j * rows : (j + 1) * rows] * score_scale), 0.0)
        denominator = jnp.sum(exponent, axis=1, keepdims=True) + own[j]
        shares.append(exponent / denominator)
        own_shares.append(own[j] / denominator)
    mixing = jnp.concatenate(
        [shares[2 * h] - lam_ref[h] * shares[2 * h + 1] for h in range(heads)], axis=0
    ).astype(BF)
    row_out = lax.broadcasted_iota(jnp.int32, (heads * rows, VD), 0) % rows
    mixed_values = jnp.zeros((heads * rows, VD), F32)
    for s in range(rows):
        product = jnp.dot(
            mixing, vc_ref[s * cache_len : (s + 1) * cache_len, :], preferred_element_type=F32
        )
        mixed_values = jnp.where(row_out == s, product, mixed_values)
    for h in range(heads):
        own_mixing = (own_shares[2 * h] - lam_ref[h] * own_shares[2 * h + 1]).astype(BF).astype(F32)
        head_out = mixed_values[h * rows : (h + 1) * rows] + own_mixing * new_value
        c_send[:, h * VD : (h + 1) * VD] = rms_scale(head_out, hgain_ref[...]).astype(BF)
    arrive(exchange(2, "ep", c_send, c_recv, False))
    d_send[...] = jnp.dot(
        stack_rows(c_recv).astype(BF), wo_ref[...], preferred_element_type=F32
    ).astype(BF)
    arrive(exchange(3, "tp", d_send, d_recv, False))
    middle = (tok_cols + jnp.sum(d_recv[...].astype(F32), axis=0)).astype(BF).astype(F32)
    gained = middle * fgain_ref[e]
    ones = jnp.ones((8, cols), F32)
    e_send[:, :seqs] = contract(ones, middle * middle, (1, 1), HI)
    e_send[:, seqs:] = contract(ones, gained * bgate_ref[e], (1, 1), HI)
    e_copies = exchange(4, "ep", e_send, e_recv, False)
    gained = gained.astype(BF)
    n_send[:, :, :half] = (
        jnp.dot(gained, wdg_ref[...], preferred_element_type=F32).reshape(n_ep, rows, half).astype(BF)
    )
    n_send[:, :, half : 2 * half] = (
        jnp.dot(gained, wdu_ref[...], preferred_element_type=F32).reshape(n_ep, rows, half).astype(BF)
    )
    n_send[:, :, 2 * half :] = middle.reshape(n_ep, rows, cols).astype(BF)
    f_send[...] = (
        contract(dispatch.astype(BF), gained, (0, 0)).reshape(n_ep, n_ep * per_dest, cols).astype(BF)
    )
    f_copies = exchange(5, "ep", f_send, f_recv, True)
    n_copies = exchange(6, "ep", n_send, n_recv, True)
    arrive(e_copies)
    stats = jnp.sum(e_recv[...], axis=0)
    scale = lax.rsqrt(stats[:, :seqs] * (1.0 / width) + epsilon)
    branch = 1.0 / (1.0 + jnp.exp(-(stats[:, seqs:] * scale)))
    first = (
        (lax.broadcasted_iota(jnp.int32, (8, 128), 0) == 0)
    ).astype(F32)
    r_rows[...] = contract(scale, first, (0, 0), HI)
    b_rows[...] = contract(branch, first, (0, 0), HI)
    r_slot[...] = contract(dispatch, r_rows[...], (0, 0), HI)
    arrive(n_copies)
    mine = pl.ds(pl.multiple_of(e * rows, rows), rows)
    r_mine = r_rows[mine, :][:, 0:1]
    both = jnp.sum(n_recv[:, :, : 2 * half].astype(F32), axis=0) * r_mine
    i_send[...] = (silu(both[:, :half]) * both[:, half:]).astype(BF)
    i_copies = exchange(7, "ep", i_send, i_recv, False)
    arrive(f_copies)
    for d in range(n_ep):
        x_all[:, d * cols : (d + 1) * cols] = f_recv[d]
    taken = n_ep * per_dest
    r_here = r_slot[pl.ds(pl.multiple_of(e * taken, taken), taken), :][:, 0:1]
    total[...] = jnp.zeros_like(total)
    owner = (lax.broadcasted_iota(jnp.int32, (taken, 1), 0) % per_dest) // CAP
    tile = 256

    def expert(h, _):
        for n, (src, dst) in enumerate(((eg_ref, eg), (eu_ref, eu), (ed_ref, ed))):
            pltpu.make_async_copy(src.at[h], dst.at[h], wsem.at[h, n]).wait()
        kept = jnp.where(owner == h, 1.0, 0.0)
        operand = x_all[...]
        for begin in range(0, hidden_here, tile):
            end = min(begin + tile, hidden_here)
            gate = jnp.dot(operand, eg[h, :, begin:end], preferred_element_type=F32) * r_here
            up = jnp.dot(operand, eu[h, :, begin:end], preferred_element_type=F32) * r_here
            unit = jnp.where(kept > 0.5, silu(gate) * up, 0.0).astype(BF)
            total[...] += jnp.dot(unit, ed[h, begin:end, :], preferred_element_type=F32)
        return 0

    lax.fori_loop(0, here, expert, 0)
    for c in range(n_tp):
        g_send[c] = total[:, c * share : (c + 1) * share].astype(BF)
    g_copies = exchange(8, "tp", g_send, g_recv, True)
    arrive(i_copies)
    product = jnp.dot(stack_rows(i_recv).astype(BF), wdd_ref[...], preferred_element_type=F32)
    j_send[...] = product.reshape(n_ep, rows, cols).astype(BF)
    j_copies = exchange(9, "ep", j_send, j_recv, True)
    arrive(g_copies)
    block_out = jnp.sum(g_recv[...].astype(F32), axis=0)
    for d in range(n_ep):
        h_send[d] = block_out[d * per_dest : (d + 1) * per_dest, :].astype(BF)
    h_copies = exchange(10, "ep", h_send, h_recv, True)
    arrive(j_copies)
    per_share = share // cols
    for d in range(n_ep):
        k_send[d // per_share, :, (d % per_share) * cols : (d % per_share + 1) * cols] = j_recv[d]
    k_copies = exchange(11, "tp", k_send, k_recv, True)
    arrive(k_copies)
    result = b_rows[mine, :][:, 0:1] * jnp.sum(k_recv[...].astype(F32), axis=0)
    mid = [n_recv[t * per_share + d][:, 2 * half :].astype(F32) for d in range(per_share)]
    result = result + jnp.concatenate(mid, axis=1)
    arrive(h_copies)
    for d in range(n_ep):
        piece = h_recv[d].astype(F32)
        for i in range(per_dest):
            q = d * per_dest + i
            result = result + combine[:, q : q + 1] * piece[i : i + 1, :]
    out_ref[...] = result.astype(BF)
    for copy in pending:
        copy.wait_send()


def fused_shards(
    tokens, norm_gain, query_weight, key_weight, value_weight, query_gain, key_gain, lambdas, key_cache,
    value_cache, lengths, head_gain, out_weight, ffn_gain, dense_gate_weight, dense_up_weight,
    dense_down_weight, branch_gate, expert_ids, expert_probs, expert_gate, expert_up, expert_down,
):
    n_ep, n_tp = lax.axis_size("ep"), lax.axis_size("tp")
    rows, width = tokens.shape
    cols = width // n_ep
    here, _, hidden_here = expert_gate.shape
    per_dest = here * CAP
    taken = n_ep * per_dest
    share = width // n_tp
    half = dense_gate_weight.shape[1]
    packed = query_weight.shape[1] + key_weight.shape[1] + value_weight.shape[1]
    seqs = n_ep * rows
    p = np.arange(n_ep * taken)
    slot_table = np.zeros((8, n_ep * taken), np.int32)
    slot_table[0] = (p // taken) * here + (p % per_dest) // CAP
    slot_table[1] = p % CAP
    slot_table[2] = (p // per_dest) % n_ep
    q = np.arange(taken)
    code_table = np.zeros((8, taken), np.int32)
    code_table[0] = (q // per_dest) * here + (q % per_dest) // CAP
    code_table[1] = q % CAP
    vmem = pl.BlockSpec(memory_space=pltpu.VMEM)
    hbm = pl.BlockSpec(memory_space=pl.ANY)
    pair = lambda shape: [pltpu.VMEM(shape, BF), pltpu.VMEM(shape, BF)]
    spread = lambda n, shape: [pltpu.VMEM(shape, BF), pltpu.VMEM((n,) + shape, BF)]
    scratch = [
        pltpu.VMEM(expert_gate.shape, BF),
        pltpu.VMEM(expert_up.shape, BF),
        pltpu.VMEM(expert_down.shape, BF),
        pltpu.VMEM((rows * key_cache.shape[2], 2 * SUB), BF),
        *pair((n_ep, rows, 2 * cols + n_ep * taken)),
        *pair((n_ep, rows, packed)),
        *spread(n_ep, (rows, out_weight.shape[0])),
        *spread(n_tp, (seqs, cols)),
        pltpu.VMEM((8, 2 * seqs), F32),
        pltpu.VMEM((n_ep, 8, 2 * seqs), F32),
        *pair((n_ep, taken, cols)),
        *pair((n_ep, rows, 2 * half + cols)),
        *spread(n_ep, (rows, half)),
        *pair((n_ep, rows, cols)),
        *pair((n_tp, rows, share)),
        *pair((n_tp, taken, share)),
        *pair((n_ep, per_dest, share)),
        pltpu.VMEM((taken, width), BF),
        pltpu.VMEM((taken, width), F32),
        pltpu.VMEM((n_ep * taken, 128), F32),
        pltpu.VMEM((seqs, 128), F32),
        pltpu.VMEM((seqs, 128), F32),
        pltpu.SemaphoreType.DMA((here, 3)),
        pltpu.SemaphoreType.DMA((12, max(n_ep, n_tp))),
        pltpu.SemaphoreType.DMA((12, max(n_ep, n_tp))),
    ]
    twice = lambda gain: jnp.concatenate([gain, gain]).reshape(1, 2 * SUB)
    return pl.pallas_call(
        functools.partial(layer_kernel, n_ep, n_tp),
        out_shape=jax.ShapeDtypeStruct((rows, share), BF),
        in_specs=[pl.BlockSpec(memory_space=pltpu.SMEM)] + [vmem] * 21 + [hbm] * 3,
        out_specs=vmem,
        scratch_shapes=scratch,
        compiler_params=pltpu.CompilerParams(
            collective_id=0, has_side_effects=True, vmem_limit_bytes=62 * 1024 * 1024
        ),
    )(
        lambdas, tokens, norm_gain.reshape(1, width), query_weight, key_weight, value_weight,
        twice(query_gain), twice(key_gain), key_cache.reshape(-1, 2 * SUB), value_cache.reshape(-1, VD),
        lengths.reshape(rows, 1), head_gain.reshape(1, VD), out_weight, ffn_gain.reshape(n_ep, 1, cols),
        dense_gate_weight, dense_up_weight, dense_down_weight, branch_gate.reshape(n_ep, 1, cols),
        expert_ids, expert_probs, jnp.asarray(slot_table), jnp.asarray(code_table),
        expert_gate, expert_up, expert_down,
    )


def dispatch_shards(*args):
    tokens, key_cache, expert_gate = args[0], args[8], args[20]
    n_ep, n_tp = lax.axis_size("ep"), lax.axis_size("tp")
    width = tokens.shape[1]
    slots = n_ep * expert_gate.shape[0]
    resident = 3 * expert_gate.size * expert_gate.dtype.itemsize
    fits = (
        slots == EXPERTS
        and key_cache.shape[1] == 1
        and tokens.shape[0] % 8 == 0
        and width % (128 * n_ep) == 0
        and (width // n_tp) % (width // n_ep) == 0
        and resident <= 40 * 1024 * 1024
    )
    return fused_shards(*args) if fits else shards(*args)


def solution(mesh):
    return jax.shard_map(
        dispatch_shards,
        mesh=mesh,
        in_specs=(
            P("ep", None),
            P(),
            P("ep", "tp"),
            P("ep", "tp"),
            P("ep", "tp"),
            P(),
            P(),
            P("tp"),
            P("ep", "tp", None, None),
            P("ep", "tp", None, None),
            P("ep"),
            P(),
            P("tp", "ep"),
            P(),
            P("ep", "tp"),
            P("ep", "tp"),
            P("tp", "ep"),
            P(),
            P("ep", None),
            P("ep", None),
            P("ep", None, "tp"),
            P("ep", None, "tp"),
            P("ep", "tp", None),
        ),
        out_specs=P("ep", "tp"),
        check_vma=False,
    )
```

profile of v0, /device:TPU:0, one launch (start us, length us, event | category | flops | bytes accessed | tf_op | source)
XLA Modules:
  0.0 56.0 jit_solution(15367553652540339741)
XLA Ops:
  0.0 1.4 %maximum_bitcast_fusion = (f32[1,128]{1,0:T(1,128)}, f32[1,128]{1,0:T(1,128)}) fusion(f32[64]{0:T(128)} %param.30, f32[64]{0:T(128)} %param.31), kind=kLoop, calls=%fused_computation | loop fusion | flops 256 | bytes 1536 | tf_op jit(solution)/shard_map/reshape | solution.py:549
  1.4 1.3 %copy.26.len_ref = s32[8,1]{1,0:T(8,128)} copy(s32[8,1]{0,1:T(1,128)} %bitcast.17) | data formatting | bytes 64 | tf_op jit(solution)/shard_map/reshape | solution.py:562
  2.7 1.3 %copy.27.ids_ref = s32[8,2]{1,0:T(8,128)} copy(s32[8,2]{0,1:T(2,128)} %param.43) | data formatting | bytes 128 | tf_op args[18]
  4.0 1.3 %copy.28.probs_ref = f32[8,2]{1,0:T(8,128)} copy(f32[8,2]{0,1:T(2,128)} %param.44) | data formatting | bytes 128 | tf_op args[19]
  5.4 49.3 %shard_map.235 = bf16[8,512]{1,0:T(8,128)(2,1)} custom-call(f32[2]{0:T(128)} %lam_ref.1, bf16[8,2048]{1,0:T(8,128)(2,1)} %tok_ref.1, f32[1,2048]{1,0:T(1,128)} %bitcast.13, bf16[256,256]{1,0:T(8,128)(2,1)} %wq_ref.1, bf16[256,128]{1,0:T(8,128)(2,1)} %wk_ref.1, bf16[256,128]{1,0:T(8,128)(2,1)} %wv_ref.1, f32[1,128]{1,0:T(1,128)} %get-tuple-element.5.qgain_ref, ...), custom_call_target="tpu_custom_call" | custom-call | tf_op jit(solution)/shard_map/pallas_call | solution.py:550
  54.7 1.3 %copy.30 = bf16[8,512]{1,0:T(8,128)(2,1)} copy(bf16[8,512]{1,0:T(8,128)(2,1)} %shard_map.235) | data formatting | bytes 16384
where the time goes:
time: 56.2 us; the launch traced here: 56 us
  Pallas kernels  49.3 us (88%)
  local copies, waits for them, and re-layouts  5.3 us (9%)
  other arithmetic  1.35 us (2%)
    pallas_call x1, Pallas kernels, fused_shards(): pl.pallas_call(functools.partial(layer_kernel, n_ep, n_tp), out_shape=jax...  49.3 us
    unnamed x3, local copies, waits for them, and re-layouts  3.98 us
    reshape x1, other arithmetic, fused_shards(): twice = lambda gain: jnp.concatenate([gain, gain]).reshape(1, 2 * SUB)  1.35 us
    reshape x1, local copies, waits for them, and re-layouts, fused_shards(): lengths.reshape(rows, 1)  1.32 us

commit v1 on v0

--- a/solution.py
+++ b/solution.py
@@ -212,6 +212,7 @@
 BF = jnp.bfloat16
 F32 = jnp.float32
 HI = lax.Precision.HIGHEST
+MESH = pl.DeviceIdType.MESH
 
 
 def contract(left, right, dims, precision=None):
@@ -224,13 +225,40 @@
     return values / (1.0 + jnp.exp(-values))
 
 
+def flip(index, bits):
+    step = 1
+    while step <= bits:
+        if bits & step:
+            index = index + step - 2 * step * ((index // step) % 2)
+        step *= 2
+    return index
+
+
+def split3(values):
+    high = values.astype(BF)
+    rest = values - high.astype(F32)
+    middle = rest.astype(BF)
+    low = (rest - middle.astype(F32)).astype(BF)
+    return [part.astype(F32) for part in (high, middle, low)]
+
+
+def in_lanes(columns, rows):
+    lane = lax.broadcasted_iota(jnp.int32, (rows, 128), 1)
+    out = jnp.zeros((rows, 128), F32)
+    for n, column in enumerate(columns):
+        out = jnp.where(lane == n, column, out)
+    return out
+
+
 def layer_kernel(
-    n_ep, n_tp, lam_ref, tok_ref, ngain_ref, wq_ref, wk_ref, wv_ref, qgain_ref, kgain_ref, kc_ref, vc_ref,
+    n_ep, n_tp, tok_hbm, ngain_hbm, wq_hbm, wk_hbm, wv_hbm, qgain_hbm, kgain_hbm, lam_hbm, kc_hbm, vc_hbm,
+    len_hbm, hgain_hbm, wo_hbm, fgain_hbm, wdg_hbm, wdu_hbm, wdd_hbm, bgate_hbm, ids_hbm, probs_hbm,
+    slot_hbm, eg_hbm, eu_hbm, ed_hbm, out_ref,
+    tok_ref, ngain_ref, wq_ref, wk_ref, wv_ref, qgain_ref, kgain_ref, lam_ref, kc_ref, vc_ref,
     len_ref, hgain_ref, wo_ref, fgain_ref, wdg_ref, wdu_ref, wdd_ref, bgate_ref, ids_ref, probs_ref,
-    slot_ref, code_ref, eg_ref, eu_ref, ed_ref, out_ref,
-    eg, eu, ed, kn, a_send, a_recv, b_send, b_recv, c_send, c_recv, d_send, d_recv, e_send, e_recv,
-    f_send, f_recv, n_send, n_recv, i_send, i_recv, j_send, j_recv, k_send, k_recv, g_send, g_recv,
-    h_send, h_recv, x_all, total, r_slot, r_rows, b_rows, wsem, ssem, rsem,
+    slot_ref, eg, eu, ed, kn, a_send, a_recv, b_send, b_recv, c_send, c_recv, f_send, f_recv, n_send,
+    n_recv, m_send, m_recv, i_send, i_recv, j_send, j_recv, g_send, g_recv, disp, acc, unit, sq,
+    lsem, wsem, ssem, rsem,
 ):
     e = lax.axis_index("ep")
     t = lax.axis_index("tp")
@@ -238,93 +266,130 @@
     cols = width // n_ep
     seqs = rows * n_ep
     here = eg.shape[0]
-    hidden_here = eg.shape[2]
     cache_len = kc_ref.shape[0] // rows
     heads = wq_ref.shape[1] // (2 * SUB)
     per_dest = here * CAP
+    taken = n_ep * per_dest
     share = width // n_tp
     half = wdg_ref.shape[1]
+    per_share = share // cols
+    far_ep = sorted(range(1, n_ep), key=lambda k: -(k % 2 + min(k // 2, n_ep // 2 - k // 2)))
+
+    barrier = pltpu.get_barrier_semaphore()
+    for k in range(1, n_ep):
+        pl.semaphore_signal(barrier, inc=1, device_id={"ep": flip(e, k)}, device_id_type=MESH)
+    for k in range(1, n_tp):
+        pl.semaphore_signal(barrier, inc=1, device_id={"tp": flip(t, k)}, device_id_type=MESH)
+
+    loads = {}
+
+    def load(name, src, dst):
+        copy = pltpu.make_async_copy(src, dst, lsem.at[len(loads)])
+        copy.start()
+        loads[name] = copy
+
+    def have(*names):
+        for name in names:
+            loads[name].wait()
+
+    load("tok", tok_hbm, tok_ref)
+    load("ids", ids_hbm, ids_ref)
+    load("kgain", kgain_hbm, kgain_ref)
+    load("kc", kc_hbm, kc_ref)
+    load("slot", slot_hbm, slot_ref)
+    load("ngain", ngain_hbm, ngain_ref)
+    load("wq", wq_hbm, wq_ref)
+    load("wk", wk_hbm, wk_ref)
+    load("wv", wv_hbm, wv_ref)
+    load("wo", wo_hbm, wo_ref.at[t])
+    load("len", len_hbm, len_ref)
+    load("probs", probs_hbm, probs_ref)
+    load("qgain", qgain_hbm, qgain_ref)
+    load("lam", lam_hbm, lam_ref)
+    load("hgain", hgain_hbm, hgain_ref)
+    load("fgain", fgain_hbm, fgain_ref)
+    load("bgate", bgate_hbm, bgate_ref)
+    load("vc", vc_hbm, vc_ref)
+    load("wdg", wdg_hbm, wdg_ref)
+    load("wdu", wdu_hbm, wdu_ref)
+    load("wdd", wdd_hbm, wdd_ref)
+
+    pending = []
+    taken_sems = [0]
+
+    def remote(src, dst, number, device, recv_number=None):
+        copy = pltpu.make_async_remote_copy(
+            src_ref=src,
+            dst_ref=dst,
+            send_sem=ssem.at[number],
+            recv_sem=rsem.at[number if recv_number is None else recv_number],
+            device_id=device,
+            device_id_type=MESH,
+        )
+        return copy
+
+    def numbers(count):
+        first = taken_sems[0]
+        taken_sems[0] += count
+        return first
+
+    def exchange(send, recv, sliced):
+        first = numbers(n_ep)
+        copies = {}
+        for k in far_ep:
+            peer = flip(e, k)
+            copy = remote(send.at[peer] if sliced else send, recv.at[e], first + k, {"ep": peer})
+            copy.start()
+            copies[k] = copy
+        pending.extend(copies.values())
+        recv[e] = send[e] if sliced else send[...]
+        return copies
+
+    def arrive(copies):
+        for copy in copies.values():
+            copy.wait_recv()
+
+    def stack_rows(values):
+        return values.astype(F32).reshape(values.shape[0] * values.shape[1], values.shape[2])
+
+    have("tok", "ids")
+    tok = tok_ref[...].astype(F32)
+    scale = lax.rsqrt(jnp.mean(tok * tok, axis=-1, keepdims=True) + epsilon)
+    eye = lax.broadcasted_iota(jnp.int32, (rows, rows), 0) == lax.broadcasted_iota(jnp.int32, (rows, rows), 1)
+    lower = lax.broadcasted_iota(jnp.int32, (rows, rows), 1) < lax.broadcasted_iota(jnp.int32, (rows, rows), 0)
+
+    def column(line):
+        return jnp.sum(jnp.where(eye, line, 0.0), axis=1, keepdims=True)
+
+    id_lines = [ids_ref[k : k + 1, :].astype(F32) for k in range(TOP)]
+    id_columns = [column(line) for line in id_lines]
+    codes = []
+    for k in range(TOP):
+        same = functools.reduce(jnp.logical_or, [id_columns[k] == line for line in id_lines])
+        rank = jnp.sum(jnp.where(jnp.logical_and(same, lower), 1.0, 0.0), axis=1, keepdims=True)
+        codes.append(id_columns[k] * CAP + rank)
+    meta = in_lanes(codes + split3(scale), rows).astype(BF)
+    for d in range(n_ep):
+        a_send[d, :, :cols] = tok_ref[:, d * cols : (d + 1) * cols]
+        a_send[d, :, cols:] = meta
 
     weight_copies = []
-    for h in range(here):
-        group = []
-        for n, (src, dst) in enumerate(((eg_ref, eg), (eu_ref, eu), (ed_ref, ed))):
+    for n, (src, dst) in enumerate(((eg_hbm, eg), (eu_hbm, eu), (ed_hbm, ed))):
+        for h in range(here):
             copy = pltpu.make_async_copy(src.at[h], dst.at[h], wsem.at[h, n])
             copy.start()
-            group.append(copy)
-        weight_copies.append(group)
-
-    barrier = pltpu.get_barrier_semaphore()
-    for k in range(1, n_ep):
-        pl.semaphore_signal(
-            barrier, inc=1, device_id={"ep": lax.rem(e + k, n_ep)}, device_id_type=pl.DeviceIdType.MESH
-        )
+            weight_copies.append(copy)
+
+    pl.semaphore_wait(barrier, n_ep - 1 + n_tp - 1)
+    a_copies = exchange(a_send, a_recv, True)
+    have("wo")
+    first = numbers(n_tp)
+    wo_copies = {}
     for k in range(1, n_tp):
-        pl.semaphore_signal(
-            barrier, inc=1, device_id={"tp": lax.rem(t + k, n_tp)}, device_id_type=pl.DeviceIdType.MESH
-        )
-
-    pending = []
-
-    def exchange(stage, axis, send, recv, sliced):
-        count, me = (n_ep, e) if axis == "ep" else (n_tp, t)
-        copies = []
-        for k in range(1, count):
-            peer = lax.rem(me + k, count)
-            copy = pltpu.make_async_remote_copy(
-                src_ref=send.at[peer] if sliced else send,
-                dst_ref=recv.at[me],
-                send_sem=ssem.at[stage, k],
-                recv_sem=rsem.at[stage, k],
-                device_id={axis: peer},
-                device_id_type=pl.DeviceIdType.MESH,
-            )
-            copy.start()
-            copies.append(copy)
-        pending.extend(copies)
-        recv[me] = send[me] if sliced else send[...]
-        return copies
-
-    def arrive(copies):
-        for copy in copies:
-            copy.wait_recv()
-
-    def stack_rows(ref):
-        values = ref[...].astype(F32)
-        return values.reshape(values.shape[0] * values.shape[1], values.shape[2])
-
-    tok = tok_ref[...].astype(F32)
-    normed = rms_scale(tok, ngain_ref[...]).astype(BF)
-    ids = ids_ref[...]
-    lower = (
-        lax.broadcasted_iota(jnp.int32, (rows, rows), 1) < lax.broadcasted_iota(jnp.int32, (rows, rows), 0)
-    ).astype(F32)
-
-    def placed(table):
-        expert = table[0:1, :]
-        hits = [(ids[:, k : k + 1] == expert).astype(F32) for k in range(TOP)]
-        named = hits[0]
-        for hit in hits[1:]:
-            named = named + hit
-        before = jnp.dot(lower, named, precision=HI, preferred_element_type=F32)
-        ranked = (before == table[1:2, :].astype(F32)).astype(F32)
-        return [hit * ranked for hit in hits]
-
-    slots = slot_ref[...]
-    marks = placed(slots)
-    chosen = functools.reduce(lambda x, y: x + y, marks) * (slots[2:3, :] == e).astype(F32)
-    chosen = chosen.astype(BF)
-    code_marks = placed(code_ref[...])
-    combine = functools.reduce(
-        lambda x, y: x + y, [code_marks[k] * probs_ref[:, k : k + 1] for k in range(TOP)]
-    )
-    tok_bf = tok_ref[...]
-    for d in range(n_ep):
-        a_send[d, :, :cols] = normed[:, d * cols : (d + 1) * cols]
-        a_send[d, :, cols : 2 * cols] = tok_bf[:, d * cols : (d + 1) * cols]
-        a_send[d, :, 2 * cols :] = chosen
-    pl.semaphore_wait(barrier, n_ep - 1 + n_tp - 1)
-    a_copies = exchange(0, "ep", a_send, a_recv, True)
+        copy = remote(wo_ref.at[t], wo_ref.at[t], first + k, {"tp": flip(t, k)})
+        copy.start()
+        wo_copies[k] = copy
+    pending.extend(wo_copies.values())
 
     lanes = 2 * SUB
     block = (
@@ -336,23 +401,45 @@
         mean = jnp.dot(values * values, block, precision=HI, preferred_element_type=F32)
         return (values * lax.rsqrt(mean + epsilon) * gain).astype(BF)
 
-    kgain = kgain_ref[...]
+    have("kgain", "kc")
+    kgain = jnp.concatenate([kgain_ref[...]] * 2, axis=1)
     for s in range(rows):
         span = slice(s * cache_len, (s + 1) * cache_len)
         kn[span, :] = parts_norm(kc_ref[span, :].astype(F32), kgain)
+    have("slot", "ngain", "wq", "wk", "wv")
 
     arrive(a_copies)
-    stacked = stack_rows(a_recv)
-    x_cols = stacked[:, :cols].astype(BF)
-    tok_cols = stacked[:, cols : 2 * cols]
-    dispatch = stacked[:, 2 * cols :]
+    stacked = stack_rows(a_recv[...])
+    tok_cols = stacked[:, :cols]
+    meta_all = stacked[:, cols:]
+    row_scale = meta_all[:, TOP : TOP + 1] + meta_all[:, TOP + 1 : TOP + 2] + meta_all[:, TOP + 2 : TOP + 3]
+    x_cols = (tok_cols * row_scale * ngain_ref[e]).astype(BF)
     start = 0
     for w_ref in (wq_ref, wk_ref, wv_ref):
         stop = start + w_ref.shape[1]
         product = jnp.dot(x_cols, w_ref[...], preferred_element_type=F32)
         b_send[:, :, start:stop] = product.reshape(n_ep, rows, stop - start).astype(BF)
         start = stop
-    arrive(exchange(1, "ep", b_send, b_recv, True))
+    b_copies = exchange(b_send, b_recv, True)
+    slots = slot_ref[...].astype(F32)
+    source = (lax.broadcasted_iota(jnp.int32, (seqs, 1), 0) // rows).astype(F32)
+    named = functools.reduce(jnp.logical_or, [meta_all[:, k : k + 1] == slots[0:1, :] for k in range(TOP)])
+    dispatch = jnp.where(jnp.logical_and(named, source == slots[1:2, :]), 1.0, 0.0).astype(BF)
+    unity = (
+        lax.broadcasted_iota(jnp.int32, (seqs, seqs), 0) == lax.broadcasted_iota(jnp.int32, (seqs, seqs), 1)
+    ).astype(BF)
+    disp[...] = contract(dispatch, unity, (0, 0)).astype(BF)
+    have("len", "probs", "qgain", "lam", "hgain", "fgain", "bgate", "vc", "wdg", "wdu", "wdd")
+    live = lax.broadcasted_iota(jnp.int32, (rows, cache_len), 1).astype(F32) < column(len_ref[...].astype(F32))
+    code_lane = lax.broadcasted_iota(jnp.int32, (rows, 128), 1).astype(F32)
+    combine = jnp.zeros((rows, 128), F32)
+    for k in range(TOP):
+        combine = combine + jnp.where(codes[k] == code_lane, column(probs_ref[k : k + 1, :]), 0.0)
+    qgain = jnp.concatenate([qgain_ref[...]] * 2, axis=1)
+    hgain = hgain_ref[...]
+    lam = [lam_ref[:, h : h + 1] for h in range(heads)]
+
+    arrive(b_copies)
     packed = jnp.sum(b_recv[...].astype(F32), axis=0).astype(BF).astype(F32)
     q_end = heads * lanes
     key_part = parts_norm(packed[:, q_end : q_end + lanes], kgain)
@@ -361,7 +448,7 @@
     score_scale = SUB ** (-0.5)
     stack, own = [], []
     for h in range(heads):
-        query = parts_norm(packed[:, h * lanes : (h + 1) * lanes], qgain_ref[...]).astype(F32)
+        query = parts_norm(packed[:, h * lanes : (h + 1) * lanes], qgain).astype(F32)
         own_pair = jnp.dot(
             query * key_part.astype(F32), block, precision=HI, preferred_element_type=F32
         ) * (SUB * score_scale)
@@ -375,7 +462,6 @@
     for s in range(rows):
         product = contract(stack, kn[s * cache_len : (s + 1) * cache_len, :], (1, 1))
         scores = jnp.where(row_of == s, product, scores)
-    live = lax.broadcasted_iota(jnp.int32, (rows, cache_len), 1) < len_ref[...]
     shares, own_shares = [], []
     for j in range(count):
         exponent = jnp.where(live, jnp.exp(scores[j * rows : (j + 1) * rows] * score_scale), 0.0)
@@ -383,7 +469,7 @@
         shares.append(exponent / denominator)
         own_shares.append(own[j] / denominator)
     mixing = jnp.concatenate(
-        [shares[2 * h] - lam_ref[h] * shares[2 * h + 1] for h in range(heads)], axis=0
+        [shares[2 * h] - lam[h] * shares[2 * h + 1] for h in range(heads)], axis=0
     ).astype(BF)
     row_out = lax.broadcasted_iota(jnp.int32, (heads * rows, VD), 0) % rows
     mixed_values = jnp.zeros((heads * rows, VD), F32)
@@ -393,102 +479,196 @@
         )
         mixed_values = jnp.where(row_out == s, product, mixed_values)
     for h in range(heads):
-        own_mixing = (own_shares[2 * h] - lam_ref[h] * own_shares[2 * h + 1]).astype(BF).astype(F32)
+        own_mixing = (own_shares[2 * h] - lam[h] * own_shares[2 * h + 1]).astype(BF).astype(F32)
         head_out = mixed_values[h * rows : (h + 1) * rows] + own_mixing * new_value
-        c_send[:, h * VD : (h + 1) * VD] = rms_scale(head_out, hgain_ref[...]).astype(BF)
-    arrive(exchange(2, "ep", c_send, c_recv, False))
-    d_send[...] = jnp.dot(
-        stack_rows(c_recv).astype(BF), wo_ref[...], preferred_element_type=F32
-    ).astype(BF)
-    arrive(exchange(3, "tp", d_send, d_recv, False))
-    middle = (tok_cols + jnp.sum(d_recv[...].astype(F32), axis=0)).astype(BF).astype(F32)
+        c_send[:, h * VD : (h + 1) * VD] = rms_scale(head_out, hgain).astype(BF)
+    first = numbers(n_ep * n_tp)
+    c_copies = {}
+    for k in far_ep + [0]:
+        for j in reversed(range(n_tp)):
+            if k or j:
+                copy = remote(
+                    c_send, c_recv.at[t, e], first + k * n_tp + j, {"ep": flip(e, k), "tp": flip(t, j)}
+                )
+                copy.start()
+                c_copies[k, j] = copy
+    pending.extend(c_copies.values())
+    c_recv[t, e] = c_send[...]
+    arrive(wo_copies)
+    arrive(c_copies)
+    middle = tok_cols
+    for c in range(n_tp):
+        product = jnp.dot(stack_rows(c_recv[c]).astype(BF), wo_ref[c], preferred_element_type=F32)
+        middle = middle + product.astype(BF).astype(F32)
+    middle_bf = middle.astype(BF)
+    middle = middle_bf.astype(F32)
+    moved = jnp.dot(disp[...], middle_bf, preferred_element_type=F32)
+    f_send[...] = moved.reshape(n_ep, taken, cols).astype(BF)
+    f_copies = exchange(f_send, f_recv, True)
     gained = middle * fgain_ref[e]
-    ones = jnp.ones((8, cols), F32)
-    e_send[:, :seqs] = contract(ones, middle * middle, (1, 1), HI)
-    e_send[:, seqs:] = contract(ones, gained * bgate_ref[e], (1, 1), HI)
-    e_copies = exchange(4, "ep", e_send, e_recv, False)
-    gained = gained.astype(BF)
+    gained_bf = gained.astype(BF)
     n_send[:, :, :half] = (
-        jnp.dot(gained, wdg_ref[...], preferred_element_type=F32).reshape(n_ep, rows, half).astype(BF)
+        jnp.dot(gained_bf, wdg_ref[...], preferred_element_type=F32).reshape(n_ep, rows, half).astype(BF)
     )
     n_send[:, :, half : 2 * half] = (
-        jnp.dot(gained, wdu_ref[...], preferred_element_type=F32).reshape(n_ep, rows, half).astype(BF)
-    )
-    n_send[:, :, 2 * half :] = middle.reshape(n_ep, rows, cols).astype(BF)
-    f_send[...] = (
-        contract(dispatch.astype(BF), gained, (0, 0)).reshape(n_ep, n_ep * per_dest, cols).astype(BF)
-    )
-    f_copies = exchange(5, "ep", f_send, f_recv, True)
-    n_copies = exchange(6, "ep", n_send, n_recv, True)
-    arrive(e_copies)
-    stats = jnp.sum(e_recv[...], axis=0)
-    scale = lax.rsqrt(stats[:, :seqs] * (1.0 / width) + epsilon)
-    branch = 1.0 / (1.0 + jnp.exp(-(stats[:, seqs:] * scale)))
-    first = (
-        (lax.broadcasted_iota(jnp.int32, (8, 128), 0) == 0)
-    ).astype(F32)
-    r_rows[...] = contract(scale, first, (0, 0), HI)
-    b_rows[...] = contract(branch, first, (0, 0), HI)
-    r_slot[...] = contract(dispatch, r_rows[...], (0, 0), HI)
+        jnp.dot(gained_bf, wdu_ref[...], preferred_element_type=F32).reshape(n_ep, rows, half).astype(BF)
+    )
+    squares = jnp.sum(middle * middle, axis=1, keepdims=True)
+    gates = jnp.sum(gained * bgate_ref[e], axis=1, keepdims=True)
+    n_send[:, :, 2 * half :] = (
+        in_lanes(split3(squares) + split3(gates), seqs).reshape(n_ep, rows, 128).astype(BF)
+    )
+    n_copies = exchange(n_send, n_recv, True)
+    m_send[...] = middle.reshape(n_ep, rows, cols).astype(BF)
+    m_first = numbers(n_ep)
+    m_slot = lax.rem(e, per_share)
+    m_copies = [
+        remote(m_send.at[flip(e, k)], m_recv.at[m_slot], m_first + k, {"ep": flip(e, k)}, m_first + m_slot)
+        for k in range(1, n_ep)
+    ]
+
+    @pl.when(t == e // per_share)
+    def _():
+        for copy in m_copies:
+            copy.start()
+        m_recv[m_slot] = m_send[e]
+
+    for copy in weight_copies[: 2 * here]:
+        copy.wait()
+
+    def chunk(k):
+        d = flip(e, k)
+        if k:
+            f_copies[k].wait_recv()
+        block_rows = pl.ds(pl.multiple_of(d * cols, cols), cols)
+        x = f_recv[d].astype(F32)
+        part = functools.reduce(
+            lambda a, b: a + b, [jnp.square(x[:, i : i + 128]) for i in range(0, cols, 128)]
+        )
+        operand = (x * fgain_ref[d]).astype(BF)
+        for h in range(here):
+            for n, ref in enumerate((eg, eu)):
+                product = jnp.dot(operand, ref[h, block_rows, :], preferred_element_type=F32)
+                if k:
+                    acc[h, n] += product
+                else:
+                    acc[h, n] = product
+        if k:
+            sq[...] += part
+        else:
+            sq[...] = part
+
+    near_ep = [0] + far_ep[::-1]
+    for k in near_ep[: n_ep - 2]:
+        chunk(k)
     arrive(n_copies)
-    mine = pl.ds(pl.multiple_of(e * rows, rows), rows)
-    r_mine = r_rows[mine, :][:, 0:1]
-    both = jnp.sum(n_recv[:, :, : 2 * half].astype(F32), axis=0) * r_mine
-    i_send[...] = (silu(both[:, :half]) * both[:, half:]).astype(BF)
-    i_copies = exchange(7, "ep", i_send, i_recv, False)
-    arrive(f_copies)
+    both = jnp.sum(n_recv[...].astype(F32), axis=0)
+    stats = both[:, 2 * half :]
+    own_scale = lax.rsqrt(
+        (stats[:, 0:1] + stats[:, 1:2] + stats[:, 2:3]) * (1.0 / width) + epsilon
+    )
+    branch = 1.0 / (1.0 + jnp.exp(-(stats[:, 3:4] + stats[:, 4:5] + stats[:, 5:6]) * own_scale))
+    scaled = both[:, : 2 * half] * own_scale
+    i_send[...] = (silu(scaled[:, :half]) * scaled[:, half:]).astype(BF)
+    i_copies = exchange(i_send, i_recv, False)
+    for k in near_ep[n_ep - 2 :]:
+        chunk(k)
+    r_here = lax.rsqrt(jnp.sum(sq[...], axis=1, keepdims=True) * (1.0 / width) + epsilon)
+    owner = (lax.broadcasted_iota(jnp.int32, (taken, 1), 0) % per_dest) // CAP
+    for h in range(here):
+        kept = owner == h
+        unit[h] = jnp.where(kept, silu(acc[h, 0] * r_here) * (acc[h, 1] * r_here), 0.0).astype(BF)
+    for copy in weight_copies[2 * here :]:
+        copy.wait()
+    g_first = numbers(n_ep * n_tp)
+    g_copies = {}
+    for j in reversed(range(n_tp)):
+        c = flip(t, j)
+        span = pl.ds(pl.multiple_of(c * share, share), share)
+        total = functools.reduce(
+            lambda a, b: a + b,
+            [jnp.dot(unit[h], ed[h, :, span], preferred_element_type=F32) for h in range(here)],
+        )
+        for d in range(n_ep):
+            g_send[j, d] = total[d * per_dest : (d + 1) * per_dest, :].astype(BF)
+        for k in far_ep + [0]:
+            if k or j:
+                peer = flip(e, k)
+                copy = remote(
+                    g_send.at[j, peer], g_recv.at[t, e], g_first + j * n_ep + k, {"ep": peer, "tp": c}
+                )
+                copy.start()
+                g_copies[j, k] = copy
+    pending.extend(g_copies.values())
+    g_recv[t, e] = g_send[0, e]
+    arrive(i_copies)
+    product = jnp.dot(stack_rows(i_recv[...]).astype(BF), wdd_ref[...], preferred_element_type=F32)
+    j_send[...] = product.reshape(n_ep, rows, cols).astype(BF)
+    j_tp = e // per_share
+    j_first = numbers(max(n_ep, n_tp * per_share))
+    j_number = j_first + t * per_share + m_slot
+    j_copies = [
+        remote(
+            j_send.at[flip(e, k)], j_recv.at[t, m_slot], j_first + k, {"ep": flip(e, k), "tp": j_tp}, j_number
+        )
+        for k in range(n_ep)
+    ]
+    for copy in j_copies[1:]:
+        copy.start()
+    pending.extend(j_copies[1:])
+
+    @pl.when(t != j_tp)
+    def _():
+        j_copies[0].start()
+
+    @pl.when(t == j_tp)
+    def _():
+        j_recv[t, m_slot] = j_send[e]
+
+    for s in range(per_share):
+        copy = remote(m_send.at[0], m_recv.at[s], m_first, {"ep": flip(e, 1)}, m_first + s)
+
+        @pl.when(t * per_share + s != e)
+        def _():
+            copy.wait_recv()
+
+    result = jnp.concatenate([m_recv[s].astype(F32) for s in range(per_share)], axis=1)
+    arrive(g_copies)
     for d in range(n_ep):
-        x_all[:, d * cols : (d + 1) * cols] = f_recv[d]
-    taken = n_ep * per_dest
-    r_here = r_slot[pl.ds(pl.multiple_of(e * taken, taken), taken), :][:, 0:1]
-    total[...] = jnp.zeros_like(total)
-    owner = (lax.broadcasted_iota(jnp.int32, (taken, 1), 0) % per_dest) // CAP
-    tile = 256
-
-    def expert(h, _):
-        for n, (src, dst) in enumerate(((eg_ref, eg), (eu_ref, eu), (ed_ref, ed))):
-            pltpu.make_async_copy(src.at[h], dst.at[h], wsem.at[h, n]).wait()
-        kept = jnp.where(owner == h, 1.0, 0.0)
-        operand = x_all[...]
-        for begin in range(0, hidden_here, tile):
-            end = min(begin + tile, hidden_here)
-            gate = jnp.dot(operand, eg[h, :, begin:end], preferred_element_type=F32) * r_here
-            up = jnp.dot(operand, eu[h, :, begin:end], preferred_element_type=F32) * r_here
-            unit = jnp.where(kept > 0.5, silu(gate) * up, 0.0).astype(BF)
-            total[...] += jnp.dot(unit, ed[h, begin:end, :], preferred_element_type=F32)
-        return 0
-
-    lax.fori_loop(0, here, expert, 0)
-    for c in range(n_tp):
-        g_send[c] = total[:, c * share : (c + 1) * share].astype(BF)
-    g_copies = exchange(8, "tp", g_send, g_recv, True)
-    arrive(i_copies)
-    product = jnp.dot(stack_rows(i_recv).astype(BF), wdd_ref[...], preferred_element_type=F32)
-    j_send[...] = product.reshape(n_ep, rows, cols).astype(BF)
-    j_copies = exchange(9, "ep", j_send, j_recv, True)
-    arrive(g_copies)
-    block_out = jnp.sum(g_recv[...].astype(F32), axis=0)
-    for d in range(n_ep):
-        h_send[d] = block_out[d * per_dest : (d + 1) * per_dest, :].astype(BF)
-    h_copies = exchange(10, "ep", h_send, h_recv, True)
-    arrive(j_copies)
-    per_share = share // cols
-    for d in range(n_ep):
-        k_send[d // per_share, :, (d % per_share) * cols : (d % per_share + 1) * cols] = j_recv[d]
-    k_copies = exchange(11, "tp", k_send, k_recv, True)
-    arrive(k_copies)
-    result = b_rows[mine, :][:, 0:1] * jnp.sum(k_recv[...].astype(F32), axis=0)
-    mid = [n_recv[t * per_share + d][:, 2 * half :].astype(F32) for d in range(per_share)]
-    result = result + jnp.concatenate(mid, axis=1)
-    arrive(h_copies)
-    for d in range(n_ep):
-        piece = h_recv[d].astype(F32)
+        piece = functools.reduce(lambda a, b: a + b, [g_recv[c, d].astype(F32) for c in range(n_tp)])
+        piece = piece.astype(BF).astype(F32)
         for i in range(per_dest):
             q = d * per_dest + i
             result = result + combine[:, q : q + 1] * piece[i : i + 1, :]
-    out_ref[...] = result.astype(BF)
+    for c in range(n_tp):
+        for s in range(per_share):
+            copy = remote(
+                j_send.at[0], j_recv.at[c, s], j_first, {"ep": flip(e, 1)}, j_first + c * per_share + s
+            )
+
+            @pl.when(jnp.logical_or(t * per_share + s != e, t != c))
+            def _():
+                copy.wait_recv()
+
+    dense = functools.reduce(
+        lambda a, b: a + b,
+        [
+            jnp.concatenate([j_recv[c, s].astype(F32) for s in range(per_share)], axis=1)
+            for c in range(n_tp)
+        ],
+    )
+    out_ref[...] = (result + branch * dense).astype(BF)
     for copy in pending:
         copy.wait_send()
+
+    @pl.when(t == e // per_share)
+    def _():
+        for copy in m_copies:
+            copy.wait_send()
+
+    @pl.when(t != j_tp)
+    def _():
+        j_copies[0].wait_send()
 
 
 def fused_shards(
@@ -503,67 +683,62 @@
     per_dest = here * CAP
     taken = n_ep * per_dest
     share = width // n_tp
+    per_share = share // cols
     half = dense_gate_weight.shape[1]
     packed = query_weight.shape[1] + key_weight.shape[1] + value_weight.shape[1]
     seqs = n_ep * rows
     p = np.arange(n_ep * taken)
     slot_table = np.zeros((8, n_ep * taken), np.int32)
-    slot_table[0] = (p // taken) * here + (p % per_dest) // CAP
-    slot_table[1] = p % CAP
-    slot_table[2] = (p // per_dest) % n_ep
-    q = np.arange(taken)
-    code_table = np.zeros((8, taken), np.int32)
-    code_table[0] = (q // per_dest) * here + (q % per_dest) // CAP
-    code_table[1] = q % CAP
+    slot_table[0] = (p // taken) * per_dest + p % per_dest
+    slot_table[1] = (p // per_dest) % n_ep
+    operands = (
+        tokens, norm_gain.reshape(n_ep, 1, cols), query_weight, key_weight, value_weight,
+        query_gain.reshape(1, SUB), key_gain.reshape(1, SUB), lambdas.reshape(1, -1),
+        key_cache.reshape(-1, 2 * SUB), value_cache.reshape(-1, VD), lengths.reshape(1, rows),
+        head_gain.reshape(1, VD), out_weight, ffn_gain.reshape(n_ep, 1, cols), dense_gate_weight,
+        dense_up_weight, dense_down_weight, branch_gate.reshape(n_ep, 1, cols), expert_ids.T,
+        expert_probs.T, jnp.asarray(slot_table), expert_gate, expert_up, expert_down,
+    )
+    local = [pltpu.VMEM(x.shape, x.dtype) for x in operands]
+    local[12] = pltpu.VMEM((n_tp,) + out_weight.shape, BF)
     vmem = pl.BlockSpec(memory_space=pltpu.VMEM)
     hbm = pl.BlockSpec(memory_space=pl.ANY)
     pair = lambda shape: [pltpu.VMEM(shape, BF), pltpu.VMEM(shape, BF)]
-    spread = lambda n, shape: [pltpu.VMEM(shape, BF), pltpu.VMEM((n,) + shape, BF)]
+    spread = lambda n, shape: [pltpu.VMEM(shape, BF), pltpu.VMEM(n + shape, BF)]
+    count = 6 * n_ep + 2 * n_ep * n_tp + n_tp + max(n_ep, n_tp * per_share)
     scratch = [
-        pltpu.VMEM(expert_gate.shape, BF),
-        pltpu.VMEM(expert_up.shape, BF),
-        pltpu.VMEM(expert_down.shape, BF),
+        *local,
         pltpu.VMEM((rows * key_cache.shape[2], 2 * SUB), BF),
-        *pair((n_ep, rows, 2 * cols + n_ep * taken)),
+        *pair((n_ep, rows, cols + 128)),
         *pair((n_ep, rows, packed)),
-        *spread(n_ep, (rows, out_weight.shape[0])),
-        *spread(n_tp, (seqs, cols)),
-        pltpu.VMEM((8, 2 * seqs), F32),
-        pltpu.VMEM((n_ep, 8, 2 * seqs), F32),
+        *spread((n_tp, n_ep), (rows, out_weight.shape[0])),
         *pair((n_ep, taken, cols)),
-        *pair((n_ep, rows, 2 * half + cols)),
-        *spread(n_ep, (rows, half)),
-        *pair((n_ep, rows, cols)),
-        *pair((n_tp, rows, share)),
-        *pair((n_tp, taken, share)),
-        *pair((n_ep, per_dest, share)),
-        pltpu.VMEM((taken, width), BF),
-        pltpu.VMEM((taken, width), F32),
-        pltpu.VMEM((n_ep * taken, 128), F32),
-        pltpu.VMEM((seqs, 128), F32),
-        pltpu.VMEM((seqs, 128), F32),
+        *pair((n_ep, rows, 2 * half + 128)),
+        pltpu.VMEM((n_ep, rows, cols), BF),
+        pltpu.VMEM((per_share, rows, cols), BF),
+        *spread((n_ep,), (rows, half)),
+        pltpu.VMEM((n_ep, rows, cols), BF),
+        pltpu.VMEM((n_tp, per_share, rows, cols), BF),
+        *pair((n_tp, n_ep, per_dest, share)),
+        pltpu.VMEM((n_ep * taken, seqs), BF),
+        pltpu.VMEM((here, 2, taken, hidden_here), F32),
+        pltpu.VMEM((here, taken, hidden_here), BF),
+        pltpu.VMEM((taken, 128), F32),
+        pltpu.SemaphoreType.DMA((24,)),
         pltpu.SemaphoreType.DMA((here, 3)),
-        pltpu.SemaphoreType.DMA((12, max(n_ep, n_tp))),
-        pltpu.SemaphoreType.DMA((12, max(n_ep, n_tp))),
+        pltpu.SemaphoreType.DMA((count,)),
+        pltpu.SemaphoreType.DMA((count,)),
     ]
-    twice = lambda gain: jnp.concatenate([gain, gain]).reshape(1, 2 * SUB)
     return pl.pallas_call(
         functools.partial(layer_kernel, n_ep, n_tp),
         out_shape=jax.ShapeDtypeStruct((rows, share), BF),
-        in_specs=[pl.BlockSpec(memory_space=pltpu.SMEM)] + [vmem] * 21 + [hbm] * 3,
+        in_specs=[hbm] * len(operands),
         out_specs=vmem,
         scratch_shapes=scratch,
         compiler_params=pltpu.CompilerParams(
             collective_id=0, has_side_effects=True, vmem_limit_bytes=62 * 1024 * 1024
         ),
-    )(
-        lambdas, tokens, norm_gain.reshape(1, width), query_weight, key_weight, value_weight,
-        twice(query_gain), twice(key_gain), key_cache.reshape(-1, 2 * SUB), value_cache.reshape(-1, VD),
-        lengths.reshape(rows, 1), head_gain.reshape(1, VD), out_weight, ffn_gain.reshape(n_ep, 1, cols),
-        dense_gate_weight, dense_up_weight, dense_down_weight, branch_gate.reshape(n_ep, 1, cols),
-        expert_ids, expert_probs, jnp.asarray(slot_table), jnp.asarray(code_table),
-        expert_gate, expert_up, expert_down,
-    )
+    )(*operands)
 
 
 def dispatch_shards(*args):
@@ -574,8 +749,11 @@
     resident = 3 * expert_gate.size * expert_gate.dtype.itemsize
     fits = (
         slots == EXPERTS
+        and n_ep & (n_ep - 1) == 0
+        and n_tp & (n_tp - 1) == 0
+        and n_ep > 2
         and key_cache.shape[1] == 1
-        and tokens.shape[0] % 8 == 0
+        and tokens.shape[0] == 8
         and width % (128 * n_ep) == 0
         and (width // n_tp) % (width // n_ep) == 0
         and resident <= 40 * 1024 * 1024

time: 56.2 us -> 41.7 us (0.74)
  Pallas kernels: 49.3 us -> 40.1 us
  local copies, waits for them, and re-layouts: 5.3 us -> 1.3 us
  other arithmetic: 1.35 us -> 0 us
    pallas_call x1, Pallas kernels: 49.3 us -> 40.1 us  [fused_shards(): pl.pallas_call(functools.partial(layer_kernel, n_ep, n_tp), out_shape=jax...]
    unnamed x3 -> x1, local copies, waits for them, and re-layouts: 3.98 us -> 1.3 us
    reshape x1 -> x0, other arithmetic: 1.35 us -> none  [fused_shards(): twice = lambda gain: jnp.concatenate([gain, gain]).reshape(1, 2 * SUB)]
    reshape x1 -> x0, local copies, waits for them, and re-layouts: 1.32 us -> none  [fused_shards(): lengths.reshape(rows, 1)]
where the time goes in v1:
time: 41.7 us; the launch traced here: 41.4 us
  Pallas kernels  40.1 us (96%)
  local copies, waits for them, and re-layouts  1.3 us (3%)
    pallas_call x1, Pallas kernels, fused_shards(): pl.pallas_call(functools.partial(layer_kernel, n_ep, n_tp), out_shape=jax...  40.1 us
    unnamed x1, local copies, waits for them, and re-layouts  1.3 us

profile of v1, /device:TPU:0, one launch (start us, length us, event | category | flops | bytes accessed | tf_op | source)
XLA Modules:
  0.0 41.4 jit_solution(14035748334147198050)
XLA Ops:
  0.0 40.1 %shard_map.226 = bf16[8,512]{1,0:T(8,128)(2,1)} custom-call(bf16[8,2048]{1,0:T(8,128)(2,1)} %tok_hbm.1, f32[8,1,256]{2,1,0:T(1,128)} %bitcast.14, bf16[256,256]{1,0:T(8,128)(2,1)} %wq_hbm.1, bf16[256,128]{1,0:T(8,128)(2,1)} %wk_hbm.1, bf16[256,128]{1,0:T(8,128)(2,1)} %wv_hbm.1, f32[1,64]{1,0:T(1,128)} %bitcast.19, f32[1,64]{1,0:T(1,128)} %bitcast.20, ...), custom_call_target="tpu_custom_call" | custom-call | tf_op jit(solution)/shard_map/pallas_call | solution.py:732
  40.1 1.3 %copy.26 = bf16[8,512]{1,0:T(8,128)(2,1)} copy(bf16[8,512]{1,0:T(8,128)(2,1)} %shard_map.226) | data formatting | bytes 16384
